TPU v7x, 32 devices: a whole 2x2x4 slice. The times are simulated.
32 devices in a mesh: sp: 16 (over z, y, core), tp: 2 (over x).
Axes of the slice: x: 2, y: 2, z: 4, core: 2. Of those that a mesh axis runs over, the one named last changes fastest.
Arguments:
- stream: bfloat16 [2048, 2048], P('sp', 'tp'), may hold values from -52 to 52
- norm_gain: float32 [2, 2048], replicated, may hold values from 0.1 to 1.9
- value_weight: bfloat16 [4096, 1024], P('sp', 'tp'), may hold values from -0.125 to 0.125
- gate_weight: bfloat16 [4096, 1024], P('sp', 'tp'), may hold values from -0.125 to 0.125
- conv_taps: float32 [2, 31, 1024], replicated, may hold values from -3 to 3
- ln_gain: float32 [2, 1024], replicated, may hold values from 0.1 to 1.9
- ln_bias: float32 [2, 1024], replicated, may hold values from -3 to 3
- out_weight: bfloat16 [1024, 4096], P('tp', 'sp'), may hold values from -0.1875 to 0.1875
- final_gain: float32 [2048], replicated, may hold values from 0.1 to 1.9
Outputs:
- result: bfloat16 [2048, 2048], P('sp', 'tp')
All inputs are finite; a program needn't handle non-finite values.
Results may differ from a plain program's by a relative error of at most 0.014.
Values may be sent and summed in bfloat16 or wider, within the bound.
A program may use at most 64 MiB of HBM per device.

v0:
```python
import jax
import jax.numpy as jnp
from jax import lax
from jax.sharding import PartitionSpec as P

D = 2048
C = 1024
KW = 31
LAYERS = 2
EPS = 1e-06


def from_behind(value, axis, steps):
    count = lax.axis_size(axis)
    first, last = (max(0, -steps), min(count, count - steps))
    return lax.ppermute(value, axis, [(source, source + steps) for source in range(first, last)])


def valid_conv(extended, tap_table):
    length = extended.shape[0] - (KW - 1)
    running = tap_table[0] * extended[0:length]
    for tap_index in range(1, KW):
        running = running + tap_table[tap_index] * extended[tap_index : tap_index + length]
    return running


def local(
    stream,
    norm_gain,
    value_weight,
    gate_weight,
    conv_taps,
    ln_gain,
    ln_bias,
    out_weight,
    final_gain,
):
    tokens_here = stream.shape[0]
    columns = stream.shape[1]
    channels = value_weight.shape[1]
    rim_rows = KW - 1
    tp_index = lax.axis_index("tp")
    my_taps = lax.dynamic_slice_in_dim(conv_taps, tp_index * channels, channels, 2)
    my_ln_gain = lax.dynamic_slice_in_dim(ln_gain, tp_index * channels, channels, 1)
    my_ln_bias = lax.dynamic_slice_in_dim(ln_bias, tp_index * channels, channels, 1)
    my_final = lax.dynamic_slice_in_dim(final_gain, tp_index * columns, columns, 0)
    value_all, gate_all, out_all = (
        lax.all_gather(value_weight, "sp", axis=0, tiled=True),
        lax.all_gather(gate_weight, "sp", axis=0, tiled=True),
        lax.all_gather(out_weight, "sp", axis=1, tiled=True),
    )
    value_all = value_all.reshape(D, LAYERS, channels)
    gate_all = gate_all.reshape(D, LAYERS, channels)
    out_all = out_all.reshape(channels, D, LAYERS)
    earlier = from_behind(stream[-LAYERS * rim_rows :], "sp", 1)
    current = jnp.concatenate([earlier, stream], axis=0)
    for layer_index in range(LAYERS):
        prefix = (LAYERS - layer_index) * rim_rows
        gathered = lax.all_gather(current, "tp", axis=1, tiled=True)
        gathered32 = gathered.astype(jnp.float32)
        scale = lax.rsqrt(jnp.sum(gathered32 * gathered32, axis=1, keepdims=True) / D + EPS)
        run_normed = (gathered32 * scale * norm_gain[layer_index]).astype(jnp.bfloat16)
        value_proj = jnp.dot(
            run_normed, value_all[:, layer_index], preferred_element_type=jnp.float32
        )
        gate_proj = jnp.dot(
            run_normed, gate_all[:, layer_index], preferred_element_type=jnp.float32
        )
        glu_out = value_proj * jax.nn.sigmoid(gate_proj)
        positions = (
            lax.axis_index("sp") * tokens_here - prefix + lax.iota(jnp.int32, current.shape[0])
        )
        extended = jnp.where((positions >= 0)[:, None], glu_out, 0.0)
        residual = current[rim_rows:].astype(jnp.float32)
        conv_out = valid_conv(extended, my_taps[layer_index])
        first_sums, square_sums = lax.psum(
            (jnp.sum(conv_out, axis=1), jnp.sum(conv_out * conv_out, axis=1)), "tp"
        )
        row_mean = (first_sums / C)[:, None]
        row_var = (square_sums / C)[:, None] - row_mean * row_mean
        run_active = jax.nn.silu(
            (conv_out - row_mean) * lax.rsqrt(row_var + EPS) * my_ln_gain[layer_index]
            + my_ln_bias[layer_index]
        ).astype(jnp.bfloat16)
        partial_value = jnp.dot(
            run_active, out_all[:, :, layer_index], preferred_element_type=jnp.float32
        )
        summed = lax.psum_scatter(
            partial_value.astype(jnp.bfloat16), "tp", scatter_dimension=1, tiled=True
        ).astype(jnp.float32)
        current = (residual + summed).astype(jnp.bfloat16)
    final32 = current.astype(jnp.float32)
    squares = lax.psum(jnp.sum(final32 * final32, axis=1), "tp")
    return (final32 * lax.rsqrt(squares[:, None] / D + EPS) * my_final).astype(jnp.bfloat16)


def solution(mesh):
    placed = (P("sp", "tp"), P(), P("sp", "tp"), P("sp", "tp"), P(), P(), P(), P("tp", "sp"), P())
    return jax.shard_map(
        local, mesh=mesh, in_specs=placed, out_specs=P("sp", "tp"), check_vma=False
    )
```

profile of v0, /device:TPU:0, one launch (start us, length us, event | category | flops | bytes accessed | tf_op | source)
XLA Modules:
  0.0 278.0 jit_solution(3715247902081535697)
XLA Ops:
  6.5 0.7 all-gather.6.cloned.1.call-update
  7.3 0.0 all-gather.4.cloned.1.call-start
  7.3 0.7 all-gather.4.cloned.1.call-update
  8.0 0.0 all-gather.8.cloned.1.call-start
  8.1 0.7 all-gather.8.cloned.1.call-update
  8.7 0.0 reduce-scatter.3.cloned.1.call-start
  8.8 0.9 slice.543
  9.7 2.4 collective-permute-start
  12.2 0.8 fusion.145
  13.0 1.0 fusion.143
  14.0 0.8 fusion.144
  14.9 1.3 constant_dynamic-slice_fusion.33
  16.2 1.0 pad_maximum_fusion
  17.2 11.7 %all_gather.15 = bf16[188,2048]{1,0:T(8,128)(2,1)S(1)} all-gather(bf16[188,1024]{1,0:T(8,128)(2,1)S(1)} %pad_maximum_fusion), channel_id=1, replica_groups=mesh['sp'=16,'tp'=2] {'tp'}, dimensions={1}, use_global_device_ids=true | all-gather | bytes 1155072 | tf_op jit(solution)/shard_map/all_gather | solution.py:59
  28.9 0.2 fusion.14
  29.1 33.5 %all-gather.6.cloned.1.call-done = bf16[4096,512]{1,0:T(8,128)(2,1)} async-done(((bf16[256,512]{1,0:T(8,128)(2,1)}), bf16[4096,512]{1,0:T(8,128)(2,1)}) %all-gather.6.cloned.1.call-update) | async-done | bytes 4194320 | tf_op jit(solution)/shard_map/all_gather | solution.py:49
  62.6 7.2 %reshape.177 = bf16[2048,2,512]{2,1,0:T(2,128)(2,1)} reshape(bf16[4096,512]{1,0:T(8,128)(2,1)} %all-gather.6.cloned.1.call-done) | data formatting | bytes 8388608 | tf_op jit(solution)/shard_map/reshape | solution.py:53
  69.8 43.9 %all-gather.4.cloned.1.call-done = bf16[4096,512]{1,0:T(8,128)(2,1)} async-done(((bf16[256,512]{1,0:T(8,128)(2,1)}), bf16[4096,512]{1,0:T(8,128)(2,1)}) %all-gather.4.cloned.1.call-update) | async-done | bytes 4194320 | tf_op jit(solution)/shard_map/all_gather | solution.py:48
  113.7 7.2 %reshape.176 = bf16[2048,2,512]{2,1,0:T(2,128)(2,1)} reshape(bf16[4096,512]{1,0:T(8,128)(2,1)} %all-gather.4.cloned.1.call-done) | data formatting | bytes 8388608 | tf_op jit(solution)/shard_map/reshape | solution.py:52
  120.9 10.0 %fusion.141 = (bf16[2048,1,512]{2,1,0:T(2,128)(2,1)}, bf16[2048,1,512]{2,1,0:T(2,128)(2,1)}) fusion(bf16[2048,2,512]{2,1,0:T(2,128)(2,1)} %reshape.177), kind=kLoop, calls=%fused_computation.233 | loop fusion | bytes 8388608 | tf_op jit(solution)/shard_map/slice | solution.py:67
  130.9 7.0 %fusion.140 = (bf16[2048,1,512]{2,1,0:T(2,128)(2,1)}, bf16[2048,1,512]{2,1,0:T(2,128)(2,1)}) fusion(bf16[2048,2,512]{2,1,0:T(2,128)(2,1)S(1)} %copy-done), kind=kLoop, calls=%fused_computation.232 | loop fusion | bytes 8388608 | tf_op jit(solution)/shard_map/slice | solution.py:64
  137.9 29.0 %all-gather.8.cloned.1.call-done = bf16[512,4096]{1,0:T(8,128)(2,1)} async-done(((bf16[512,256]{1,0:T(8,128)(2,1)}), bf16[512,4096]{1,0:T(8,128)(2,1)}) %all-gather.8.cloned.1.call-update) | async-done | bytes 4194320 | tf_op jit(solution)/shard_map/all_gather | solution.py:50
  166.9 6.5 %copy.13 = bf16[512,4096]{0,1:T(8,128)(2,1)} copy(bf16[512,4096]{1,0:T(8,128)(2,1)} %all-gather.8.cloned.1.call-done) | data formatting | bytes 8388608 | tf_op jit(solution)/shard_map/all_gather | solution.py:50
  173.4 7.2 %reshape.178 = bf16[512,2048,2]{0,2,1:T(2,128)(2,1)} reshape(bf16[512,4096]{0,1:T(8,128)(2,1)} %copy.13) | data formatting | bytes 8388608 | tf_op jit(solution)/shard_map/reshape | solution.py:54
  180.6 9.9 %fusion.142 = (bf16[512,2048,1]{0,2,1:T(2,128)(2,1)}, bf16[512,2048,1]{0,2,1:T(2,128)(2,1)}) fusion(bf16[512,2048,2]{0,2,1:T(2,128)(2,1)} %reshape.178), kind=kLoop, calls=%fused_computation.234 | loop fusion | bytes 8388608 | tf_op jit(solution)/shard_map/slice | solution.py:86
  190.5 9.0 %copy.14 = bf16[512,2048,1]{1,0,2:T(8,128)(2,1)S(1)} copy(bf16[512,2048,1]{0,2,1:T(2,128)(2,1)} %get-tuple-element.19) | data formatting | bytes 4194304 | tf_op jit(solution)/shard_map/slice | solution.py:86
  199.5 3.0 %fusion.29 = f32[188,512]{1,0:T(8,128)S(1)} fusion(bf16[2048,1,512]{2,1,0:T(2,128)(2,1)} %get-tuple-element.17, bf16[188,2048]{1,0:T(8,128)(2,1)S(1)} %all_gather.15, f32[2048]{0:T(1024)S(1)} %bitcast.145, f32[188]{0:T(256)S(1)} %add_rsqrt_fusion.2), kind=kOutput, calls=%fused_computation.29 | convolution fusion | flops 396093440 | bytes 3261168 | tf_op jit(solution)/shard_map/dot_general | solution.py:66
  202.6 0.4 copy-done.2
  203.0 0.6 fusion.35
  203.6 1.5 fusion.136
  205.1 4.9 %all-reduce.1 = (f32[158]{0:T(256)S(1)}, f32[158]{0:T(256)S(1)}) all-reduce(f32[158]{0:T(256)S(1)} %get-tuple-element.6, f32[158]{0:T(256)S(1)} %get-tuple-element.5), channel_id=1, replica_groups=mesh['sp'=16,'tp'=2] {'tp'}, use_global_device_ids=true, to_apply=%region_4.5 | all-reduce | flops 316 | bytes 2528 | tf_op jit(solution)/shard_map/psum | solution.py:76
  210.0 1.5 convolution_convert_fusion
  211.6 0.0 reduce-scatter.5.cloned.1.call-start
  211.7 9.1 %copy.15 = bf16[512,2048,1]{1,0,2:T(8,128)(2,1)S(1)} copy(bf16[512,2048,1]{0,2,1:T(2,128)(2,1)} %get-tuple-element.20) | data formatting | bytes 4194304 | tf_op jit(solution)/shard_map/slice | solution.py:86
  220.7 5.3 %reduce-scatter.3.cloned.1.call-done = bf16[158,1024]{1,0:T(8,128)(2,1)} async-done(((bf16[158,2048]{1,0:T(8,128)(2,1)}), bf16[158,1024]{1,0:T(8,128)(2,1)}) %reduce-scatter.3.cloned.1.call-update) | async-done | bytes 323600 | tf_op jit(solution)/shard_map/reduce_scatter | solution.py:88
  226.0 1.1 add_convert_fusion
  227.1 9.9 %all_gather.19 = bf16[158,2048]{1,0:T(8,128)(2,1)S(1)} all-gather(bf16[158,1024]{1,0:T(8,128)(2,1)S(1)} %add_convert_fusion), channel_id=1, replica_groups=mesh['sp'=16,'tp'=2] {'tp'}, dimensions={1}, use_global_device_ids=true | all-gather | bytes 970752 | tf_op jit(solution)/shard_map/all_gather | solution.py:59
  237.0 0.2 fusion.17
  237.3 3.0 %fusion.50 = f32[158,512]{1,0:T(8,128)S(1)} fusion(bf16[2048,1,512]{2,1,0:T(2,128)(2,1)} %get-tuple-element.18, bf16[158,2048]{1,0:T(8,128)(2,1)S(1)} %all_gather.19, f32[2048]{0:T(1024)S(1)} %bitcast.143, f32[158]{0:T(256)S(1)} %add_rsqrt_fusion), kind=kOutput, calls=%fused_computation.36 | convolution fusion | flops 332887040 | bytes 3076728 | tf_op jit(solution)/shard_map/dot_general | solution.py:66
  240.2 0.5 copy-done.1
  240.7 0.6 fusion.53
  241.3 1.1 fusion.137
  242.4 4.9 %all-reduce = (f32[128]{0:T(128)S(1)}, f32[128]{0:T(128)S(1)}) all-reduce(f32[128]{0:T(128)S(1)} %get-tuple-element.8, f32[128]{0:T(128)S(1)} %get-tuple-element.7), channel_id=1, replica_groups=mesh['sp'=16,'tp'=2] {'tp'}, use_global_device_ids=true, to_apply=%region_10.11 | all-reduce | flops 256 | bytes 2048 | tf_op jit(solution)/shard_map/psum | solution.py:76
  247.4 1.3 convolution_convert_fusion.1
  248.8 14.8 %reduce-scatter.5.cloned.1.call-done = bf16[128,1024]{1,0:T(8,128)(2,1)} async-done(((bf16[128,2048]{1,0:T(8,128)(2,1)}), bf16[128,1024]{1,0:T(8,128)(2,1)}) %reduce-scatter.5.cloned.1.call-update) | async-done | bytes 262160 | tf_op jit(solution)/shard_map/reduce_scatter | solution.py:88
  263.6 1.2 fusion.56
  264.7 4.9 %psum.39 = f32[128]{0:T(128)S(1)} all-reduce(f32[128]{0:T(128)S(1)} %fusion.56), channel_id=1, replica_groups=mesh['sp'=16,'tp'=2] {'tp'}, use_global_device_ids=true, to_apply=%region_13.14 | all-reduce | flops 128 | bytes 1024 | tf_op jit(solution)/shard_map/psum | solution.py:93
  269.6 1.8 fusion.58
  (20 shorter events, 0.1 us)
Async XLA Ops:
  6.5 56.1 %all-gather.6.cloned.1.call-start = ((), (), s32[]{:S(2)}) async-start(), calls=%async_computation.3 | async-start | bytes 4456448 | tf_op jit(solution)/shard_map/all_gather | solution.py:49
  7.3 106.5 %all-gather.4.cloned.1.call-start = ((), (), s32[]{:S(2)}) async-start(), calls=%async_computation.2 | async-start | bytes 4456448 | tf_op jit(solution)/shard_map/all_gather | solution.py:48
  8.0 158.9 %all-gather.8.cloned.1.call-start = ((), (), s32[]{:S(2)}) async-start(), calls=%async_computation.4 | async-start | bytes 4456448 | tf_op jit(solution)/shard_map/all_gather | solution.py:50
  8.7 217.3 %reduce-scatter.3.cloned.1.call-start = ((), (), s32[]{:S(2)}) async-start(), calls=%async_computation.5 | async-start | bytes 983040 | tf_op jit(solution)/shard_map/reduce_scatter | solution.py:88
  9.7 6.4 %collective-permute-start = (bf16[60,1024]{1,0:T(8,128)(2,1)S(1)}, bf16[60,1024]{1,0:T(8,128)(2,1)S(1)}, u32[]{:S(2)}, u32[]{:S(2)}) collective-permute-start(bf16[60,1024]{1,0:T(8,128)(2,1)S(1)} %slice.543), channel_id=1, source_target_pairs={{0,2},{2,4},{4,6},{6,8},{8,10},{10,12},{12,14},{14,16},{16,18},{18... | collective-permute-start | bytes 368648 | tf_op jit(solution)/shard_map/ppermute | solution.py:16
  120.9 10.0 %copy-start = (bf16[2048,2,512]{2,1,0:T(2,128)(2,1)S(1)}, bf16[2048,2,512]{2,1,0:T(2,128)(2,1)}, u32[]{:S(2)}) copy-start(bf16[2048,2,512]{2,1,0:T(2,128)(2,1)} %reshape.176) | copy-start | bytes 12582916
  199.5 3.5 %copy-start.2 = (bf16[2048,1,512]{2,1,0:T(2,128)(2,1)S(1)}, bf16[2048,1,512]{2,1,0:T(2,128)(2,1)}, u32[]{:S(2)}) copy-start(bf16[2048,1,512]{2,1,0:T(2,128)(2,1)} %get-tuple-element.16) | copy-start | bytes 6291460
  211.6 52.0 %reduce-scatter.5.cloned.1.call-start = ((), (), s32[]{:S(2)}) async-start(), calls=%async_computation.6 | async-start | bytes 786432 | tf_op jit(solution)/shard_map/reduce_scatter | solution.py:88
  211.7 14.3 %copy-start.3 = (bf16[128,1024]{1,0:T(8,128)(2,1)S(1)}, bf16[128,1024]{1,0:T(8,128)(2,1)}, u32[]{:S(2)}) copy-start(bf16[128,1024]{1,0:T(8,128)(2,1)} %param.9) | copy-start | bytes 786436
  237.2 3.5 %copy-start.1 = (bf16[2048,1,512]{2,1,0:T(2,128)(2,1)S(1)}, bf16[2048,1,512]{2,1,0:T(2,128)(2,1)}, u32[]{:S(2)}) copy-start(bf16[2048,1,512]{2,1,0:T(2,128)(2,1)} %get-tuple-element.15) | copy-start | bytes 6291460
  242.4 6.3 %copy-start.4 = (f32[2048]{0:T(1024)S(1)}, f32[2048]{0:T(1024)}, u32[]{:S(2)}) copy-start(f32[2048]{0:T(1024)} %param.17) | copy-start | bytes 24580
Sparse Core Ops, SparseCore 0:
  9.5 53.0 all-gather.5
  64.8 48.8 all-gather.3
  115.9 50.9 all-gather.7
  211.7 14.2 reduce-scatter.2
  248.8 14.6 reduce-scatter.4
where the time goes:
time: 279 us; the launch traced here: 278 us
  waiting for transfers between devices  129 us (46%)
  local copies, waits for them, and re-layouts  78.9 us (28%)
  blocking collectives  36.4 us (13%)
  between operations  13.3 us (5%)
  matrix products  10 us (4%)
  other arithmetic  8.25 us (3%)
    all_gather x1, waiting for transfers between devices, local(): lax.all_gather(value_weight, 'sp', axis=0, tiled=True)  43.9 us
    all_gather x1, waiting for transfers between devices, local(): lax.all_gather(gate_weight, 'sp', axis=0, tiled=True)  33.5 us
    all_gather x1, waiting for transfers between devices, local(): lax.all_gather(out_weight, 'sp', axis=1, tiled=True)  29 us
    slice x3, local copies, waits for them, and re-layouts, local(): out_all[:, :, layer_index]  28 us
    all_gather x2, blocking collectives, local(): gathered = lax.all_gather(current, 'tp', axis=1, tiled=True)  21.6 us
    reduce_scatter x2, waiting for transfers between devices, local(): lax.psum_scatter(partial_value.astype(jnp.bfloat16), 'tp', scatter_dimens...  20.1 us
    slice x1, local copies, waits for them, and re-layouts, local(): gate_all[:, layer_index]  9.98 us
    psum x2, blocking collectives, local(): lax.psum((jnp.sum(conv_out, axis=1), jnp.sum(conv_out * conv_out, axis=1)...  9.87 us
  transfers between devices with their start and end apart: 6, of which 5 were waited for; matrix products, arithmetic and copies ran while one was open for 17% of the time, Pallas kernels for 0%

commit v1 on v0

--- a/solution.py
+++ b/solution.py
@@ -56,7 +56,7 @@
     current = jnp.concatenate([earlier, stream], axis=0)
     for layer_index in range(LAYERS):
         prefix = (LAYERS - layer_index) * rim_rows
-        gathered = lax.all_gather(current, "tp", axis=1, tiled=True)
+        gathered = jnp.concatenate(lax.all_gather(current, "tp"), axis=1)
         gathered32 = gathered.astype(jnp.float32)
         scale = lax.rsqrt(jnp.sum(gathered32 * gathered32, axis=1, keepdims=True) / D + EPS)
         run_normed = (gathered32 * scale * norm_gain[layer_index]).astype(jnp.bfloat16)

time: 279 us -> 281 us (level)
  local copies, waits for them, and re-layouts: 78.9 us -> 83.5 us
    unnamed x10 -> x16, local copies, waits for them, and re-layouts: 0.92 us -> 4.16 us
where the time goes in v1:
time: 281 us; the launch traced here: 279 us
  waiting for transfers between devices  127 us (45%)
  local copies, waits for them, and re-layouts  83.5 us (30%)
  blocking collectives  36.6 us (13%)
  between operations  13.4 us (5%)
  other arithmetic  8.73 us (3%)
  matrix products  7.5 us (3%)
    all_gather x1, waiting for transfers between devices, local(): lax.all_gather(value_weight, 'sp', axis=0, tiled=True)  43.9 us
    all_gather x1, waiting for transfers between devices, local(): lax.all_gather(gate_weight, 'sp', axis=0, tiled=True)  31.6 us
    all_gather x1, waiting for transfers between devices, local(): lax.all_gather(out_weight, 'sp', axis=1, tiled=True)  29.2 us
    slice x3, local copies, waits for them, and re-layouts, local(): out_all[:, :, layer_index]  28 us
    all_gather x2, blocking collectives, local(): gathered = jnp.concatenate(lax.all_gather(current, 'tp'), axis=1)  21.8 us
    reduce_scatter x2, waiting for transfers between devices, local(): lax.psum_scatter(partial_value.astype(jnp.bfloat16), 'tp', scatter_dimens...  20 us
    psum x2, blocking collectives, local(): lax.psum((jnp.sum(conv_out, axis=1), jnp.sum(conv_out * conv_out, axis=1)...  9.87 us
    slice x1, local copies, waits for them, and re-layouts, local(): gate_all[:, layer_index]  9.81 us
  transfers between devices with their start and end apart: 6, of which 5 were waited for; matrix products, arithmetic and copies ran while one was open for 17% of the time, Pallas kernels for 0%

profile of v1, /device:TPU:0, one launch (start us, length us, event | category | flops | bytes accessed | tf_op | source)
XLA Modules:
  0.0 279.0 jit_solution(6128244267186683800)
XLA Ops:
  6.5 0.7 all-gather.10.cloned.1.call-update
  7.3 0.7 all-gather.8.cloned.1.call-update
  8.1 0.7 all-gather.12.cloned.1.call-update
  8.8 0.9 slice.543
  9.7 2.4 collective-permute-start
  12.2 0.8 fusion.143
  13.0 1.0 fusion.142
  14.0 0.8 slice_reduce_fusion
  14.9 1.3 constant_dynamic-slice_fusion.33
  16.2 1.0 fusion.61
  17.2 11.7 %all-gather.2 = bf16[2,188,1024]{2,1,0:T(8,128)(2,1)S(1)} all-gather(bf16[1,188,1024]{2,1,0:T(8,128)(2,1)S(1)} %fusion.61), channel_id=2, replica_groups=mesh['sp'=16,'tp'=2] {'tp'}, dimensions={0}, use_global_device_ids=true | all-gather | bytes 1155072 | tf_op jit(solution)/shard_map/all_gather | solution.py:59
  29.1 0.3 fusion.56
  29.4 0.8 copy.20
  30.2 0.6 pad.2
  31.0 31.6 %all-gather.10.cloned.1.call-done = bf16[4096,512]{1,0:T(8,128)(2,1)} async-done(((bf16[256,512]{1,0:T(8,128)(2,1)}), bf16[4096,512]{1,0:T(8,128)(2,1)}) %all-gather.10.cloned.1.call-update) | async-done | bytes 4194320 | tf_op jit(solution)/shard_map/all_gather | solution.py:49
  62.6 7.2 %reshape.225 = bf16[2048,2,512]{2,1,0:T(2,128)(2,1)} reshape(bf16[4096,512]{1,0:T(8,128)(2,1)} %all-gather.10.cloned.1.call-done) | data formatting | bytes 8388608 | tf_op jit(solution)/shard_map/reshape | solution.py:53
  69.8 43.9 %all-gather.8.cloned.1.call-done = bf16[4096,512]{1,0:T(8,128)(2,1)} async-done(((bf16[256,512]{1,0:T(8,128)(2,1)}), bf16[4096,512]{1,0:T(8,128)(2,1)}) %all-gather.8.cloned.1.call-update) | async-done | bytes 4194320 | tf_op jit(solution)/shard_map/all_gather | solution.py:48
  113.7 7.2 %reshape.224 = bf16[2048,2,512]{2,1,0:T(2,128)(2,1)} reshape(bf16[4096,512]{1,0:T(8,128)(2,1)} %all-gather.8.cloned.1.call-done) | data formatting | bytes 8388608 | tf_op jit(solution)/shard_map/reshape | solution.py:52
  120.9 9.8 %fusion.140 = (bf16[2048,1,512]{2,1,0:T(2,128)(2,1)}, bf16[2048,1,512]{2,1,0:T(2,128)(2,1)}) fusion(bf16[2048,2,512]{2,1,0:T(2,128)(2,1)} %reshape.225), kind=kLoop, calls=%fused_computation.238 | loop fusion | bytes 8388608 | tf_op jit(solution)/shard_map/slice | solution.py:67
  130.8 7.0 %fusion.139 = (bf16[2048,1,512]{2,1,0:T(2,128)(2,1)}, bf16[2048,1,512]{2,1,0:T(2,128)(2,1)}) fusion(bf16[2048,2,512]{2,1,0:T(2,128)(2,1)S(1)} %copy-done), kind=kLoop, calls=%fused_computation.237 | loop fusion | bytes 8388608 | tf_op jit(solution)/shard_map/slice | solution.py:64
  137.8 29.2 %all-gather.12.cloned.1.call-done = bf16[512,4096]{1,0:T(8,128)(2,1)} async-done(((bf16[512,256]{1,0:T(8,128)(2,1)}), bf16[512,4096]{1,0:T(8,128)(2,1)}) %all-gather.12.cloned.1.call-update) | async-done | bytes 4194320 | tf_op jit(solution)/shard_map/all_gather | solution.py:50
  166.9 6.5 %copy.21 = bf16[512,4096]{0,1:T(8,128)(2,1)} copy(bf16[512,4096]{1,0:T(8,128)(2,1)} %all-gather.12.cloned.1.call-done) | data formatting | bytes 8388608 | tf_op jit(solution)/shard_map/all_gather | solution.py:50
  173.4 7.2 %reshape.226 = bf16[512,2048,2]{0,2,1:T(2,128)(2,1)} reshape(bf16[512,4096]{0,1:T(8,128)(2,1)} %copy.21) | data formatting | bytes 8388608 | tf_op jit(solution)/shard_map/reshape | solution.py:54
  180.6 9.9 %fusion.141 = (bf16[512,2048,1]{0,2,1:T(2,128)(2,1)}, bf16[512,2048,1]{0,2,1:T(2,128)(2,1)}) fusion(bf16[512,2048,2]{0,2,1:T(2,128)(2,1)} %reshape.226), kind=kLoop, calls=%fused_computation.239 | loop fusion | bytes 8388608 | tf_op jit(solution)/shard_map/slice | solution.py:86
  190.5 9.0 %copy.22 = bf16[512,2048,1]{1,0,2:T(8,128)(2,1)S(1)} copy(bf16[512,2048,1]{0,2,1:T(2,128)(2,1)} %get-tuple-element.21) | data formatting | bytes 4194304 | tf_op jit(solution)/shard_map/slice | solution.py:86
  199.5 3.0 %fusion.29 = f32[188,512]{1,0:T(8,128)S(1)} fusion(bf16[188,2048]{1,0:T(8,128)(2,1)S(1)} %bitcast.130, bf16[2048,1,512]{2,1,0:T(2,128)(2,1)} %get-tuple-element.20), kind=kOutput, calls=%fused_computation.29 | convolution fusion | flops 394553344 | bytes 3252224 | tf_op jit(solution)/shard_map/dot_general | solution.py:66
  202.5 0.5 copy-done.3
  203.0 0.6 fusion.35
  203.6 1.5 fusion.135
  205.1 4.9 %all-reduce.1 = (f32[158]{0:T(256)S(1)}, f32[158]{0:T(256)S(1)}) all-reduce(f32[158]{0:T(256)S(1)} %get-tuple-element.6, f32[158]{0:T(256)S(1)} %get-tuple-element.5), channel_id=1, replica_groups=mesh['sp'=16,'tp'=2] {'tp'}, use_global_device_ids=true, to_apply=%region_4.5 | all-reduce | flops 316 | bytes 2528 | tf_op jit(solution)/shard_map/psum | solution.py:76
  210.0 1.5 convolution_convert_fusion
  211.7 9.1 %copy.24 = bf16[512,2048,1]{1,0,2:T(8,128)(2,1)S(1)} copy(bf16[512,2048,1]{0,2,1:T(2,128)(2,1)} %get-tuple-element.22) | data formatting | bytes 4194304 | tf_op jit(solution)/shard_map/slice | solution.py:86
  220.7 5.2 %reduce-scatter.3.cloned.1.call-done = bf16[158,1024]{1,0:T(8,128)(2,1)} async-done(((bf16[158,2048]{1,0:T(8,128)(2,1)}), bf16[158,1024]{1,0:T(8,128)(2,1)}) %reduce-scatter.3.cloned.1.call-update) | async-done | bytes 323600 | tf_op jit(solution)/shard_map/reduce_scatter | solution.py:88
  226.0 1.1 add_convert_fusion
  227.1 10.1 %all-gather.3 = bf16[2,158,1024]{2,1,0:T(8,128)(2,1)S(1)} all-gather(bf16[1,158,1024]{2,1,0:T(8,128)(2,1)S(1)} %bitcast.127), channel_id=3, replica_groups=mesh['sp'=16,'tp'=2] {'tp'}, dimensions={0}, use_global_device_ids=true | all-gather | bytes 970752 | tf_op jit(solution)/shard_map/all_gather | solution.py:59
  237.7 0.7 copy.23
  238.3 0.5 pad.3
  239.0 0.6 copy-done.1
  239.6 0.6 fusion.50
  240.2 1.6 copy-done.2
  241.8 0.5 fusion.53
  242.3 1.1 fusion.136
  243.5 4.9 %all-reduce = (f32[128]{0:T(128)S(1)}, f32[128]{0:T(128)S(1)}) all-reduce(f32[128]{0:T(128)S(1)} %get-tuple-element.8, f32[128]{0:T(128)S(1)} %get-tuple-element.7), channel_id=1, replica_groups=mesh['sp'=16,'tp'=2] {'tp'}, use_global_device_ids=true, to_apply=%region_10.11 | all-reduce | flops 256 | bytes 2048 | tf_op jit(solution)/shard_map/psum | solution.py:76
  248.4 1.4 convolution_convert_fusion.1
  249.8 14.8 %reduce-scatter.5.cloned.1.call-done = bf16[128,1024]{1,0:T(8,128)(2,1)} async-done(((bf16[128,2048]{1,0:T(8,128)(2,1)}), bf16[128,1024]{1,0:T(8,128)(2,1)}) %reduce-scatter.5.cloned.1.call-update) | async-done | bytes 262160 | tf_op jit(solution)/shard_map/reduce_scatter | solution.py:88
  264.6 1.2 fusion.58
  265.8 4.9 %psum.39 = f32[128]{0:T(128)S(1)} all-reduce(f32[128]{0:T(128)S(1)} %fusion.58), channel_id=1, replica_groups=mesh['sp'=16,'tp'=2] {'tp'}, use_global_device_ids=true, to_apply=%region_13.14 | all-reduce | flops 128 | bytes 1024 | tf_op jit(solution)/shard_map/psum | solution.py:93
  270.7 1.8 fusion.60
  (32 shorter events, 1.3 us)
Async XLA Ops:
  6.5 56.1 %all-gather.10.cloned.1.call-start = ((), (), s32[]{:S(2)}) async-start(), calls=%async_computation.3 | async-start | bytes 4456448 | tf_op jit(solution)/shard_map/all_gather | solution.py:49
  7.3 106.5 %all-gather.8.cloned.1.call-start = ((), (), s32[]{:S(2)}) async-start(), calls=%async_computation.2 | async-start | bytes 4456448 | tf_op jit(solution)/shard_map/all_gather | solution.py:48
  8.0 158.9 %all-gather.12.cloned.1.call-start = ((), (), s32[]{:S(2)}) async-start(), calls=%async_computation.4 | async-start | bytes 4456448 | tf_op jit(solution)/shard_map/all_gather | solution.py:50
  8.7 217.2 %reduce-scatter.3.cloned.1.call-start = ((), (), s32[]{:S(2)}) async-start(), calls=%async_computation.5 | async-start | bytes 983040 | tf_op jit(solution)/shard_map/reduce_scatter | solution.py:88
  9.7 6.5 %collective-permute-start = (bf16[60,1024]{1,0:T(8,128)(2,1)S(1)}, bf16[60,1024]{1,0:T(8,128)(2,1)S(1)}, u32[]{:S(2)}, u32[]{:S(2)}) collective-permute-start(bf16[60,1024]{1,0:T(8,128)(2,1)S(1)} %slice.543), channel_id=1, source_target_pairs={{0,2},{2,4},{4,6},{6,8},{8,10},{10,12},{12,14},{14,16},{16,18},{18... | collective-permute-start | bytes 368648 | tf_op jit(solution)/shard_map/ppermute | solution.py:16
  120.9 9.8 %copy-start = (bf16[2048,2,512]{2,1,0:T(2,128)(2,1)S(1)}, bf16[2048,2,512]{2,1,0:T(2,128)(2,1)}, u32[]{:S(2)}) copy-start(bf16[2048,2,512]{2,1,0:T(2,128)(2,1)} %reshape.224) | copy-start | bytes 12582916
  199.5 3.5 %copy-start.3 = (bf16[2048,1,512]{2,1,0:T(2,128)(2,1)S(1)}, bf16[2048,1,512]{2,1,0:T(2,128)(2,1)}, u32[]{:S(2)}) copy-start(bf16[2048,1,512]{2,1,0:T(2,128)(2,1)} %get-tuple-element.18) | copy-start | bytes 6291460
  211.6 53.0 %reduce-scatter.5.cloned.1.call-start = ((), (), s32[]{:S(2)}) async-start(), calls=%async_computation.6 | async-start | bytes 786432 | tf_op jit(solution)/shard_map/reduce_scatter | solution.py:88
  211.6 14.3 %copy-start.4 = (bf16[128,1024]{1,0:T(8,128)(2,1)S(1)}, bf16[128,1024]{1,0:T(8,128)(2,1)}, u32[]{:S(2)}) copy-start(bf16[128,1024]{1,0:T(8,128)(2,1)} %param.9) | copy-start | bytes 786436
  237.4 2.2 copy-start.1
  239.6 2.2 copy-start.2
  243.5 6.3 %copy-start.5 = (f32[2048]{0:T(1024)S(1)}, f32[2048]{0:T(1024)}, u32[]{:S(2)}) copy-start(f32[2048]{0:T(1024)} %param.17) | copy-start | bytes 24580
Sparse Core Ops, SparseCore 0:
  9.5 53.0 all-gather.9
  64.8 48.8 all-gather.7
  115.9 50.9 all-gather.11
  211.7 14.2 reduce-scatter.2
  249.9 14.6 reduce-scatter.4
